TPU v7x, 32 devices: a whole 2x2x4 slice. The times are simulated.
32 devices in a mesh: fs: 8 (over z, x), tp: 4 (over y, core).
Axes of the slice: x: 2, y: 2, z: 4, core: 2. Of those that a mesh axis runs over, the one named last changes fastest.
Arguments:
- tokens: bfloat16 [4096, 2048], P('fs', 'tp'), may hold values from -6 to 6
- pre_gain: float32 [2048], replicated, may hold values from 0.1 to 1.9
- pre_gate: float32 [2048, 2816], P('fs', 'tp'), may hold values from -0.125 to 0.125
- pre_up: float32 [2048, 2816], P('fs', 'tp'), may hold values from -0.125 to 0.125
- pre_down: float32 [2816, 2048], P('fs', 'tp'), may hold values from -0.109375 to 0.109375
- mix_gain: float32 [2048], replicated, may hold values from 0.1 to 1.9
- branch_proj: float32 [2048, 1024], P('fs', 'tp'), may hold values from -0.125 to 0.125
- gate_proj: float32 [2048, 1024], P('fs', 'tp'), may hold values from -0.125 to 0.125
- conv_taps: float32 [4, 1024], P(None, 'tp'), may hold values from -3 to 3
- retain_blocks: float32 [16, 64, 64], P('tp'), may hold values from -0.75 to 0.75
- admit_blocks: float32 [16, 64, 64], P('tp'), may hold values from -0.75 to 0.75
- decay_param: float32 [1024], P('tp'), may hold values from 5 to 8.5
- channel_gain: float32 [1024], replicated, may hold values from 0.1 to 1.9
- out_proj: float32 [1024, 2048], P('fs', 'tp'), may hold values from -0.1875 to 0.1875
- post_gain: float32 [2048], replicated, may hold values from 0.1 to 1.9
- post_gate: float32 [2048, 2816], P('fs', 'tp'), may hold values from -0.125 to 0.125
- post_up: float32 [2048, 2816], P('fs', 'tp'), may hold values from -0.125 to 0.125
- post_down: float32 [2816, 2048], P('fs', 'tp'), may hold values from -0.109375 to 0.109375
Outputs:
- layer_out: bfloat16 [4096, 2048], P('fs', 'tp')
All inputs are finite; a program needn't handle non-finite values.
Results may differ from a plain program's by a relative error of at most 0.012.
Values may be sent and summed in bfloat16 or wider, within the bound.
A program may use at most 64 MiB of HBM per device.

v0:
```python
import jax
import jax.numpy as jnp
from jax import lax
from jax.sharding import PartitionSpec as P

SEQ_LEN = 128
EPSILON = 1e-06
DECAY_SCALE = 8.0


def normalize(values, norm_gain):
    floats = values.astype(jnp.float32)
    scaled = floats * lax.rsqrt(jnp.mean(floats * floats, axis=-1, keepdims=True) + EPSILON)
    return (scaled * norm_gain).astype(jnp.bfloat16)


def combine(earlier, latter):
    keep_early, add_early = earlier
    keep_late, add_late = latter
    return (keep_early * keep_late, keep_late * add_early + add_late)


def widen(residual):
    return lax.all_gather(residual, "tp", axis=1, tiled=True)


def contract(operand, stacked):
    return jnp.dot(
        operand,
        lax.all_gather(stacked.astype(jnp.bfloat16), "fs", axis=0, tiled=True),
        preferred_element_type=jnp.float32,
    )


def feed_forward(residual, norm_gain, gate_matrix, up_matrix, down_matrix):
    normed = normalize(widen(residual), norm_gain)
    products = contract(normed, jnp.concatenate((gate_matrix, up_matrix), axis=1))
    split_at = gate_matrix.shape[1]
    hidden = (jax.nn.silu(products[:, :split_at]) * products[:, split_at:]).astype(jnp.bfloat16)
    all_hidden = lax.all_gather(hidden, "tp", axis=1, tiled=True)
    return (residual.astype(jnp.float32) + 0.5 * contract(all_hidden, down_matrix)).astype(
        jnp.bfloat16
    )


def block_gate(convolved, blocks):
    grouped = convolved.reshape(
        convolved.shape[0], convolved.shape[1], blocks.shape[0], blocks.shape[1]
    )
    mixed = jnp.einsum(
        "sthi,hij->sthj", grouped, blocks.astype(jnp.bfloat16), preferred_element_type=jnp.float32
    )
    return jax.nn.sigmoid(mixed).reshape(convolved.shape)


def recurrent_mixer(
    residual,
    norm_gain,
    branch_matrix,
    gate_matrix,
    conv_taps,
    retain_blocks,
    admit_blocks,
    decay_param,
    channel_gain,
    out_matrix,
):
    normed = normalize(widen(residual), norm_gain)
    products = contract(normed, jnp.concatenate((branch_matrix, gate_matrix), axis=1))
    local_width = branch_matrix.shape[1]
    branch = products[:, :local_width]
    gate_act = products[:, local_width:]
    taps_count = conv_taps.shape[0]
    sequences = residual.shape[0] // SEQ_LEN
    framed = branch.reshape(sequences, SEQ_LEN, local_width)
    padded = jnp.pad(framed, ((0, 0), (taps_count - 1, 0), (0, 0)))
    convolved = jnp.zeros_like(framed)
    for tap_index in range(taps_count):
        convolved = convolved + padded[:, tap_index : tap_index + SEQ_LEN] * conv_taps[tap_index]
    convolved = convolved.astype(jnp.bfloat16)
    retained = block_gate(convolved, retain_blocks)
    admitted = block_gate(convolved, admit_blocks)
    log_keep = -DECAY_SCALE * retained * jax.nn.softplus(-decay_param)
    inject = jnp.sqrt(-jnp.expm1(2.0 * log_keep)) * admitted * convolved.astype(jnp.float32)
    _, states = lax.associative_scan(combine, (jnp.exp(log_keep), inject), axis=1)
    mixed_rows = (states.reshape(residual.shape[0], local_width) * jax.nn.gelu(gate_act)).astype(
        jnp.bfloat16
    )
    all_channels = lax.all_gather(mixed_rows, "tp", axis=1, tiled=True)
    mixed_normed = normalize(all_channels, channel_gain)
    return (residual.astype(jnp.float32) + contract(mixed_normed, out_matrix)).astype(jnp.bfloat16)


def local(
    tokens,
    pre_gain,
    pre_gate,
    pre_up,
    pre_down,
    mix_gain,
    branch_proj,
    gate_proj,
    conv_taps,
    retain_blocks,
    admit_blocks,
    decay_param,
    channel_gain,
    out_proj,
    post_gain,
    post_gate,
    post_up,
    post_down,
):
    after_pre = feed_forward(tokens, pre_gain, pre_gate, pre_up, pre_down)
    after_mix = recurrent_mixer(
        after_pre,
        mix_gain,
        branch_proj,
        gate_proj,
        conv_taps,
        retain_blocks,
        admit_blocks,
        decay_param,
        channel_gain,
        out_proj,
    )
    return feed_forward(after_mix, post_gain, post_gate, post_up, post_down)


def solution(mesh):
    placed = (
        P("fs", "tp"),
        P(),
        P("fs", "tp"),
        P("fs", "tp"),
        P("fs", "tp"),
        P(),
        P("fs", "tp"),
        P("fs", "tp"),
        P(None, "tp"),
        P("tp", None, None),
        P("tp", None, None),
        P("tp"),
        P(),
        P("fs", "tp"),
        P(),
        P("fs", "tp"),
        P("fs", "tp"),
        P("fs", "tp"),
    )
    return jax.shard_map(
        local, mesh=mesh, in_specs=placed, out_specs=P("fs", "tp"), check_vma=False
    )
```

profile of v0, /device:TPU:0, one launch (start us, length us, event | category | flops | bytes accessed | tf_op | source)
XLA Modules:
  0.0 807.1 jit_solution(914277624177452306)
XLA Ops:
  10.4 23.8 %all-gather.13.cloned.1.call-done = bf16[512,2048]{1,0:T(8,128)(2,1)} async-done(((bf16[512,512]{1,0:T(8,128)(2,1)}), bf16[512,2048]{1,0:T(8,128)(2,1)}) %all-gather.13.cloned.1.call-update) | async-done | bytes 2097168 | tf_op jit(solution)/shard_map/all_gather | solution.py:24
  34.2 2.2 fusion
  36.5 93.0 %all-gather.15.cloned.1.call-done = bf16[2048,1408]{0,1:T(8,128)(2,1)} async-done(((bf16[256,1408]{0,1:T(8,128)(2,1)}), bf16[2048,1408]{0,1:T(8,128)(2,1)}) %all-gather.15.cloned.1.call-update) | async-done | bytes 5767184 | tf_op jit(solution)/shard_map/all_gather | solution.py:30
  129.4 5.8 fusion.16
  137.0 50.1 %all-gather.19.cloned.1.call-done = bf16[2816,512]{1,0:T(8,128)(2,1)} async-done(((bf16[352,512]{1,0:T(8,128)(2,1)}), bf16[2816,512]{1,0:T(8,128)(2,1)}) %all-gather.19.cloned.1.call-update) | async-done | bytes 2883600 | tf_op jit(solution)/shard_map/all_gather | solution.py:30
  187.1 27.1 %all-gather.17.cloned.1.call-done = bf16[512,2816]{0,1:T(8,128)(2,1)} async-done(((bf16[512,704]{0,1:T(8,128)(2,1)}), bf16[512,2816]{0,1:T(8,128)(2,1)}) %all-gather.17.cloned.1.call-update) | async-done | bytes 2883600 | tf_op jit(solution)/shard_map/all_gather | solution.py:40
  214.2 5.2 fusion.29
  220.4 21.7 %all-gather.21.cloned.1.call-done = bf16[512,2048]{1,0:T(8,128)(2,1)} async-done(((bf16[512,512]{1,0:T(8,128)(2,1)}), bf16[512,2048]{1,0:T(8,128)(2,1)}) %all-gather.21.cloned.1.call-update) | async-done | bytes 2097168 | tf_op jit(solution)/shard_map/all_gather | solution.py:24
  242.1 2.2 fusion.3
  244.4 48.9 %all-gather.23.cloned.1.call-done = bf16[2048,512]{1,0:T(8,128)(2,1)} async-done(((bf16[256,512]{1,0:T(8,128)(2,1)}), bf16[2048,512]{1,0:T(8,128)(2,1)}) %all-gather.23.cloned.1.call-update) | async-done | bytes 2097168 | tf_op jit(solution)/shard_map/all_gather | solution.py:30
  293.2 2.9 fusion.14
  299.5 9.1 %slice.212 = f32[4,64,256]{1,2,0:T(8,128)S(1)} slice(f32[4,128,256]{1,2,0:T(8,128)S(1)} %get-tuple-element.6), slice={[0:4:1], [0:127:2], [0:256:1]} | slice | bytes 524288 | tf_op jit(solution)/shard_map/slice | solution.py:85
  308.6 9.1 %slice.213 = f32[4,64,256]{1,2,0:T(8,128)S(1)} slice(f32[4,128,256]{1,2,0:T(8,128)S(1)} %get-tuple-element.6), slice={[0:4:1], [1:128:2], [0:256:1]} | slice | bytes 524288 | tf_op jit(solution)/shard_map/slice | solution.py:85
  317.6 9.1 %slice.211 = f32[4,64,256]{1,2,0:T(8,128)S(1)} slice(f32[4,128,256]{1,2,0:T(8,128)S(1)} %get-tuple-element.5), slice={[0:4:1], [1:128:2], [0:256:1]} | slice | bytes 524288 | tf_op jit(solution)/shard_map/slice | solution.py:85
  326.7 9.5 %slice.215 = f32[4,64,256]{1,2,0:T(8,128)} slice(f32[4,128,256]{1,2,0:T(8,128)S(1)} %get-tuple-element.5), slice={[0:4:1], [0:127:2], [0:256:1]} | slice | bytes 524288 | tf_op jit(solution)/shard_map/slice | solution.py:85
  337.4 4.6 slice.218
  342.0 4.7 slice.219
  346.7 5.3 slice.217
  352.1 5.2 slice.221
  358.6 2.5 slice.224
  361.0 3.2 slice.225
  364.2 3.4 slice.223
  367.6 3.1 slice.227
  372.2 2.3 slice.230
  374.4 2.4 slice.231
  376.8 2.4 slice.229
  379.2 2.3 slice.233
  385.0 2.0 slice.237
  386.9 2.0 slice.235
  390.7 2.4 fusion.72
  396.6 3.4 slice.241
  400.0 3.3 slice.245
  408.7 3.5 slice.234
  414.0 3.7 slice.228
  417.8 2.3 slice.253
  420.0 3.1 slice.222
  423.1 3.1 slice.255
  426.2 6.1 slice.216
  432.2 5.2 slice.257
  437.4 9.5 %slice.259 = f32[4,63,256]{1,2,0:T(8,128)} slice(f32[4,128,256]{1,2,0:T(8,128)S(1)} %get-tuple-element.6), slice={[0:4:1], [2:128:2], [0:256:1]} | slice | bytes 516096 | tf_op jit(solution)/shard_map/slice | solution.py:85
  446.9 9.9 %slice.210 = f32[4,63,256]{1,2,0:T(8,128)} slice(f32[4,128,256]{1,2,0:T(8,128)S(1)} %copy-done.1), slice={[0:4:1], [2:128:2], [0:256:1]} | slice | bytes 516096 | tf_op jit(solution)/shard_map/slice | solution.py:85
  461.6 2.2 pad.50
  463.8 4.3 pad.51
  470.0 2.5 pad.53
  472.4 2.2 add_multiply_fusion.4
  478.4 2.4 pad.52
  481.7 1.9 add_multiply_fusion.3
  487.7 2.9 pad.55
  491.5 3.7 pad.57
  497.5 3.6 pad.56
  502.3 4.5 pad.58
  506.8 4.6 pad.59
  512.3 9.8 %pad.61 = f32[4,128,256]{1,2,0:T(8,128)S(1)} pad(f32[4,64,256]{1,2,0:T(8,128)} %add.195, f32[]{:T(128)} %constant.10.clone.1), padding=0_0_0x1_0_1x0_0_0 | pad | bytes 786436 | tf_op jit(solution)/shard_map/pad | solution.py:85
  522.5 8.8 %pad.60 = f32[4,128,256]{1,2,0:T(8,128)S(1)} pad(f32[4,64,256]{1,2,0:T(8,128)S(1)} %pad_maximum_fusion.4, f32[]{:T(128)} %constant.10.clone.1), padding=0_0_0x0_1_1x0_0_0 | pad | bytes 786436 | tf_op jit(solution)/shard_map/pad | solution.py:85
  533.3 14.7 %all-gather.25.cloned.1.call-done = bf16[512,1024]{1,0:T(8,128)(2,1)} async-done(((bf16[512,256]{1,0:T(8,128)(2,1)}), bf16[512,1024]{1,0:T(8,128)(2,1)}) %all-gather.25.cloned.1.call-update) | async-done | bytes 1048592 | tf_op jit(solution)/shard_map/all_gather | solution.py:89
  549.6 40.9 %all-gather.27.cloned.1.call-done = bf16[1024,512]{1,0:T(8,128)(2,1)} async-done(((bf16[128,512]{1,0:T(8,128)(2,1)}), bf16[1024,512]{1,0:T(8,128)(2,1)}) %all-gather.27.cloned.1.call-update) | async-done | bytes 1048592 | tf_op jit(solution)/shard_map/all_gather | solution.py:30
  590.5 3.1 fusion.30
  595.8 19.2 %all-gather.29.cloned.1.call-done = bf16[512,2048]{1,0:T(8,128)(2,1)} async-done(((bf16[512,512]{1,0:T(8,128)(2,1)}), bf16[512,2048]{1,0:T(8,128)(2,1)}) %all-gather.29.cloned.1.call-update) | async-done | bytes 2097168 | tf_op jit(solution)/shard_map/all_gather | solution.py:24
  615.0 2.2 fusion.6
  617.3 92.8 %all-gather.31.cloned.1.call-done = bf16[2048,1408]{0,1:T(8,128)(2,1)} async-done(((bf16[256,1408]{0,1:T(8,128)(2,1)}), bf16[2048,1408]{0,1:T(8,128)(2,1)}) %all-gather.31.cloned.1.call-update) | async-done | bytes 5767184 | tf_op jit(solution)/shard_map/all_gather | solution.py:30
  710.1 5.8 fusion.12
  717.6 50.2 %all-gather.35.cloned.1.call-done = bf16[2816,512]{1,0:T(8,128)(2,1)} async-done(((bf16[352,512]{1,0:T(8,128)(2,1)}), bf16[2816,512]{1,0:T(8,128)(2,1)}) %all-gather.35.cloned.1.call-update) | async-done | bytes 2883600 | tf_op jit(solution)/shard_map/all_gather | solution.py:30
  767.8 27.1 %all-gather.33.cloned.1.call-done = bf16[512,2816]{0,1:T(8,128)(2,1)} async-done(((bf16[512,704]{0,1:T(8,128)(2,1)}), bf16[512,2816]{0,1:T(8,128)(2,1)}) %all-gather.33.cloned.1.call-update) | async-done | bytes 2883600 | tf_op jit(solution)/shard_map/all_gather | solution.py:40
  794.9 5.2 fusion.28
  (181 shorter events, 57.9 us)
Async XLA Ops:
  6.5 2.0 copy-start.21
  6.5 27.7 %all-gather.13.cloned.1.call-start = ((), (), s32[]{:S(2)}) async-start(), calls=%async_computation | async-start | bytes 2621440 | tf_op jit(solution)/shard_map/all_gather | solution.py:24
  7.3 2.3 copy-start.22
  7.3 122.1 %all-gather.15.cloned.1.call-start = ((), (), s32[]{:S(2)}) async-start(), calls=%async_computation.1 | async-start | bytes 6488064 | tf_op jit(solution)/shard_map/all_gather | solution.py:30
  9.5 119.9 %copy-start.36 = (f32[2048]{0:T(1024)S(1)}, f32[2048]{0:T(1024)}, u32[]{:S(2)}) copy-start(f32[2048]{0:T(1024)} %param.19) | copy-start | bytes 24580
  9.5 177.6 %all-gather.19.cloned.1.call-start = ((), (), s32[]{:S(2)}) async-start(), calls=%async_computation.3 | async-start | bytes 3244032 | tf_op jit(solution)/shard_map/all_gather | solution.py:30
  10.4 203.8 %all-gather.17.cloned.1.call-start = ((), (), s32[]{:S(2)}) async-start(), calls=%async_computation.2 | async-start | bytes 3604480 | tf_op jit(solution)/shard_map/all_gather | solution.py:40
  34.2 95.2 %copy-start.14 = (bf16[512,2048]{1,0:T(8,128)(2,1)S(1)}, bf16[512,2048]{1,0:T(8,128)(2,1)}, u32[]{:S(2)}) copy-start(bf16[512,2048]{1,0:T(8,128)(2,1)} %all-gather.13.cloned.1.call-done) | copy-start | bytes 6291460
  135.8 78.4 %copy-start.26 = (bf16[512,512]{1,0:T(8,128)(2,1)S(1)}, bf16[512,512]{1,0:T(8,128)(2,1)}, u32[]{:S(2)}) copy-start(bf16[512,512]{1,0:T(8,128)(2,1)} %param.18) | copy-start | bytes 1572868
  136.9 82.5 %copy-start.29 = (f32[256,256]{1,0:T(8,128)S(1)}, f32[256,256]{1,0:T(8,128)}, u32[]{:S(2)}) copy-start(f32[256,256]{1,0:T(8,128)} %param.24) | copy-start | bytes 786436
  137.0 82.5 %copy-start.30 = (f32[256,256]{1,0:T(8,128)S(1)}, f32[256,256]{1,0:T(8,128)}, u32[]{:S(2)}) copy-start(f32[256,256]{1,0:T(8,128)} %param.25) | copy-start | bytes 786436
  137.0 105.2 %all-gather.21.cloned.1.call-start = ((), (), s32[]{:S(2)}) async-start(), calls=%async_computation.4 | async-start | bytes 2621440 | tf_op jit(solution)/shard_map/all_gather | solution.py:24
  219.4 1.0 copy-start.33
  219.4 1.0 copy-start.32
  219.4 73.8 %copy-start.37 = (f32[2048]{0:T(1024)S(1)}, f32[2048]{0:T(1024)}, u32[]{:S(2)}) copy-start(f32[2048]{0:T(1024)} %param.23) | copy-start | bytes 24580
  219.4 73.8 %all-gather.23.cloned.1.call-start = ((), (), s32[]{:S(2)}) async-start(), calls=%async_computation.5 | async-start | bytes 2359296 | tf_op jit(solution)/shard_map/all_gather | solution.py:30
  220.3 327.7 %all-gather.25.cloned.1.call-start = ((), (), s32[]{:S(2)}) async-start(), calls=%async_computation.6 | async-start | bytes 1310720 | tf_op jit(solution)/shard_map/all_gather | solution.py:89
  242.1 51.1 %copy-start.16 = (bf16[512,2048]{1,0:T(8,128)(2,1)S(1)}, bf16[512,2048]{1,0:T(8,128)(2,1)}, u32[]{:S(2)}) copy-start(bf16[512,2048]{1,0:T(8,128)(2,1)} %all-gather.21.cloned.1.call-done) | copy-start | bytes 6291460
  296.1 1.0 copy-start.19
  296.1 1.8 copy-start.34
  297.3 1.0 copy-start.35
  299.4 27.2 %copy-start = (f32[4,128,256]{1,2,0:T(8,128)}, f32[4,128,256]{1,2,0:T(8,128)S(1)}, u32[]{:S(2)}) copy-start(f32[4,128,256]{1,2,0:T(8,128)S(1)} %get-tuple-element.5) | copy-start | bytes 1572868
  337.4 14.7 %copy-start.2 = (f32[4,64,256]{1,2,0:T(8,128)}, f32[4,64,256]{1,2,0:T(8,128)S(1)}, u32[]{:S(2)}) copy-start(f32[4,64,256]{1,2,0:T(8,128)S(1)} %get-tuple-element.19) | copy-start | bytes 786436
  358.6 9.1 %copy-start.3 = (f32[4,32,256]{1,2,0:T(8,128)}, f32[4,32,256]{1,2,0:T(8,128)S(1)}, u32[]{:S(2)}) copy-start(f32[4,32,256]{1,2,0:T(8,128)S(1)} %get-tuple-element.17) | copy-start | bytes 393220
  372.2 7.0 copy-start.5
  383.1 5.8 copy-start.6
  403.3 1.5 copy-start.9
  403.3 1.7 copy-start.18
  405.0 1.0 copy-start.7
  408.7 11.4 %copy-start.4 = (f32[4,32,256]{1,2,0:T(8,128)S(1)}, f32[4,32,256]{1,2,0:T(8,128)}, u32[]{:S(2)}) copy-start(f32[4,32,256]{1,2,0:T(8,128)} %copy-done.3) | copy-start | bytes 393220
  423.1 23.8 %copy-start.1 = (f32[4,128,256]{1,2,0:T(8,128)S(1)}, f32[4,128,256]{1,2,0:T(8,128)}, u32[]{:S(2)}) copy-start(f32[4,128,256]{1,2,0:T(8,128)} %copy-done) | copy-start | bytes 1572868
  463.7 4.3 copy-start.8
  496.5 5.5 copy-start.12
  496.5 5.5 copy-start.13
  502.1 4.7 copy-start.17
  506.8 15.3 %copy-start.10 = (f32[4,63,256]{1,2,0:T(8,128)S(1)}, f32[4,63,256]{1,2,0:T(8,128)}, u32[]{:S(2)}) copy-start(f32[4,63,256]{1,2,0:T(8,128)} %slice.259) | copy-start | bytes 774148
  506.8 15.3 %copy-start.11 = (f32[4,63,256]{1,2,0:T(8,128)S(1)}, f32[4,63,256]{1,2,0:T(8,128)}, u32[]{:S(2)}) copy-start(f32[4,63,256]{1,2,0:T(8,128)} %slice.210) | copy-start | bytes 774148
  522.5 9.1 %copy-start.20 = (f32[512,512]{1,0:T(8,128)S(1)}, f32[512,512]{1,0:T(8,128)}, u32[]{:S(2)}) copy-start(f32[512,512]{1,0:T(8,128)} %copy-done.19) | copy-start | bytes 3145732
  531.3 1.3 copy-start.31
  531.4 59.1 %copy-start.27 = (bf16[512,512]{1,0:T(8,128)(2,1)S(1)}, bf16[512,512]{1,0:T(8,128)(2,1)}, u32[]{:S(2)}) copy-start(bf16[512,512]{1,0:T(8,128)(2,1)} %fusion.29) | copy-start | bytes 1572868
  531.4 59.1 %copy-start.39 = (f32[1024]{0:T(1024)S(1)}, f32[1024]{0:T(1024)}, u32[]{:S(2)}) copy-start(f32[1024]{0:T(1024)} %param.30) | copy-start | bytes 12292
  532.5 57.9 %all-gather.27.cloned.1.call-start = ((), (), s32[]{:S(2)}) async-start(), calls=%async_computation.7 | async-start | bytes 1179648 | tf_op jit(solution)/shard_map/all_gather | solution.py:30
  533.3 81.7 %all-gather.29.cloned.1.call-start = ((), (), s32[]{:S(2)}) async-start(), calls=%async_computation.8 | async-start | bytes 2621440 | tf_op jit(solution)/shard_map/all_gather | solution.py:24
  549.5 44.3 %copy-start.23 = (f32[256,704]{0,1:T(8,128)S(1)}, f32[256,704]{0,1:T(8,128)}, u32[]{:S(2)}) copy-start(f32[256,704]{0,1:T(8,128)} %param.33) | copy-start | bytes 2162692
  549.6 44.3 %copy-start.24 = (f32[256,704]{0,1:T(8,128)S(1)}, f32[256,704]{0,1:T(8,128)}, u32[]{:S(2)}) copy-start(f32[256,704]{0,1:T(8,128)} %param.34) | copy-start | bytes 2162692
  593.6 1.3 copy-start.25
  593.6 116.5 %all-gather.31.cloned.1.call-start = ((), (), s32[]{:S(2)}) async-start(), calls=%async_computation.9 | async-start | bytes 6488064 | tf_op jit(solution)/shard_map/all_gather | solution.py:30
  594.9 115.2 %copy-start.38 = (f32[2048]{0:T(1024)S(1)}, f32[2048]{0:T(1024)}, u32[]{:S(2)}) copy-start(f32[2048]{0:T(1024)} %param.32) | copy-start | bytes 24580
  594.9 172.9 %all-gather.35.cloned.1.call-start = ((), (), s32[]{:S(2)}) async-start(), calls=%async_computation.11 | async-start | bytes 3244032 | tf_op jit(solution)/shard_map/all_gather | solution.py:30
  595.8 199.1 %all-gather.33.cloned.1.call-start = ((), (), s32[]{:S(2)}) async-start(), calls=%async_computation.10 | async-start | bytes 3604480 | tf_op jit(solution)/shard_map/all_gather | solution.py:40
  615.0 95.1 %copy-start.15 = (bf16[512,2048]{1,0:T(8,128)(2,1)S(1)}, bf16[512,2048]{1,0:T(8,128)(2,1)}, u32[]{:S(2)}) copy-start(bf16[512,2048]{1,0:T(8,128)(2,1)} %all-gather.29.cloned.1.call-done) | copy-start | bytes 6291460
  716.4 78.5 %copy-start.28 = (bf16[512,512]{1,0:T(8,128)(2,1)S(1)}, bf16[512,512]{1,0:T(8,128)(2,1)}, u32[]{:S(2)}) copy-start(bf16[512,512]{1,0:T(8,128)(2,1)} %fusion.30) | copy-start | bytes 1572868
Sparse Core Ops, SparseCore 0:
  8.9 25.2 all-gather.12
  36.3 93.1 all-gather.14
  131.6 55.4 all-gather.18
  188.5 25.6 all-gather.16
  219.5 22.5 all-gather.20
  244.1 49.0 all-gather.22
  532.6 15.3 all-gather.24
  550.2 40.2 all-gather.26
  593.7 21.2 all-gather.28
  616.9 93.1 all-gather.30
  712.3 55.4 all-gather.34
  769.2 25.6 all-gather.32
where the time goes:
time: 815 us; the launch traced here: 807 us
  waiting for transfers between devices  510 us (63%)
  local copies, waits for them, and re-layouts  210 us (26%)
  other arithmetic  42.7 us (5%)
  matrix products  28.7 us (4%)
  between operations  14.5 us (2%)
    all_gather x6, waiting for transfers between devices, contract(): lax.all_gather(stacked.astype(jnp.bfloat16), 'fs', axis=0, tiled=True)  376 us
    slice x34, local copies, waits for them, and re-layouts, recurrent_mixer(): lax.associative_scan(combine, (jnp.exp(log_keep), inject), axis=1)  144 us
    all_gather x3, waiting for transfers between devices, widen(): return lax.all_gather(residual, 'tp', axis=1, tiled=True)  64.7 us
    all_gather x2, waiting for transfers between devices, feed_forward(): all_hidden = lax.all_gather(hidden, 'tp', axis=1, tiled=True)  54.2 us
    pad x12, local copies, waits for them, and re-layouts, recurrent_mixer(): lax.associative_scan(combine, (jnp.exp(log_keep), inject), axis=1)  50.5 us
    dot_general x6, matrix products, contract(): jnp.dot(operand, lax.all_gather(stacked.astype(jnp.bfloat16), 'fs', axis=...  28 us
  transfers between devices with their start and end apart: 12, of which 12 were waited for; matrix products, arithmetic and copies ran while one was open for 4% of the time, Pallas kernels for 0%

commit v1 on v0

--- a/solution.py
+++ b/solution.py
@@ -37,7 +37,12 @@
     products = contract(normed, jnp.concatenate((gate_matrix, up_matrix), axis=1))
     split_at = gate_matrix.shape[1]
     hidden = (jax.nn.silu(products[:, :split_at]) * products[:, split_at:]).astype(jnp.bfloat16)
-    all_hidden = lax.all_gather(hidden, "tp", axis=1, tiled=True)
+    ring = [hidden]
+    for hop in range(3):
+        ring.append(lax.ppermute(ring[-1], "tp", [(dev, (dev + 1) % 4) for dev in range(4)]))
+    all_hidden = jnp.roll(
+        jnp.concatenate(ring[::-1], axis=1), (lax.axis_index("tp") + 1) * ring[0].shape[1], axis=1
+    )
     return (residual.astype(jnp.float32) + 0.5 * contract(all_hidden, down_matrix)).astype(
         jnp.bfloat16
     )

time: 815 us -> 764 us (0.937)
  waiting for transfers between devices: 510 us -> 443 us
  local copies, waits for them, and re-layouts: 210 us -> 219 us
    all_gather x6, waiting for transfers between devices: 376 us -> 302 us  [contract(): lax.all_gather(stacked.astype(jnp.bfloat16), 'fs', axis=0, tiled=True)]
    ppermute x0 -> x6, waiting for transfers between devices: none -> 63.3 us  [feed_forward(): lax.ppermute(ring[-1], 'tp', [(dev, (dev + 1) % 4) for dev in range(4)])]
    all_gather x2 -> x0, waiting for transfers between devices: 54.2 us -> none  [feed_forward(): all_hidden = lax.all_gather(hidden, 'tp', axis=1, tiled=True)]
  transfers between devices with their start and end apart: 12 -> 16, of which waited for: 12 -> 16; matrix products, arithmetic and copies ran while one was open for 4% -> 5% of each run, Pallas kernels for 0% -> 0%
where the time goes in v1:
time: 764 us; the launch traced here: 754 us
  waiting for transfers between devices  443 us (58%)
  local copies, waits for them, and re-layouts  219 us (29%)
  other arithmetic  44.4 us (6%)
  matrix products  32.6 us (4%)
  between operations  14.5 us (2%)
    all_gather x6, waiting for transfers between devices, contract(): lax.all_gather(stacked.astype(jnp.bfloat16), 'fs', axis=0, tiled=True)  302 us
    slice x34, local copies, waits for them, and re-layouts, recurrent_mixer(): lax.associative_scan(combine, (jnp.exp(log_keep), inject), axis=1)  144 us
    ppermute x6, waiting for transfers between devices, feed_forward(): lax.ppermute(ring[-1], 'tp', [(dev, (dev + 1) % 4) for dev in range(4)])  63.3 us
    all_gather x3, waiting for transfers between devices, widen(): return lax.all_gather(residual, 'tp', axis=1, tiled=True)  62.4 us
    pad x12, local copies, waits for them, and re-layouts, recurrent_mixer(): lax.associative_scan(combine, (jnp.exp(log_keep), inject), axis=1)  50.4 us
    dot_general x6, matrix products, contract(): jnp.dot(operand, lax.all_gather(stacked.astype(jnp.bfloat16), 'fs', axis=...  31.9 us
  transfers between devices with their start and end apart: 16, of which 16 were waited for; matrix products, arithmetic and copies ran while one was open for 5% of the time, Pallas kernels for 0%

profile of v1, /device:TPU:0, one launch (start us, length us, event | category | flops | bytes accessed | tf_op | source)
XLA Modules:
  0.0 754.1 jit_solution(11978213390054257925)
XLA Ops:
  11.5 22.7 %all-gather.11.cloned.1.call-done = bf16[512,2048]{1,0:T(8,128)(2,1)} async-done(((bf16[512,512]{1,0:T(8,128)(2,1)}), bf16[512,2048]{1,0:T(8,128)(2,1)}) %all-gather.11.cloned.1.call-update) | async-done | bytes 2097168 | tf_op jit(solution)/shard_map/all_gather | solution.py:24
  36.3 93.1 %all-gather.13.cloned.1.call-done = bf16[2048,1408]{0,1:T(8,128)(2,1)} async-done(((bf16[256,1408]{0,1:T(8,128)(2,1)}), bf16[2048,1408]{0,1:T(8,128)(2,1)}) %all-gather.13.cloned.1.call-update) | async-done | bytes 5767184 | tf_op jit(solution)/shard_map/all_gather | solution.py:30
  129.4 6.5 fusion.22
  136.8 10.7 %collective-permute-done = bf16[512,704]{0,1:T(8,128)(2,1)S(1)} collective-permute-done((bf16[512,704]{0,1:T(8,128)(2,1)S(1)}, bf16[512,704]{0,1:T(8,128)(2,1)S(1)}, u32[]{:S(2)}, u32[]{:S(2)}) %collective-permute-start) | collective-permute-done | bytes 720928 | tf_op jit(solution)/shard_map/ppermute | solution.py:42
  147.5 10.7 %collective-permute-done.1 = bf16[512,704]{0,1:T(8,128)(2,1)S(1)} collective-permute-done((bf16[512,704]{0,1:T(8,128)(2,1)S(1)}, bf16[512,704]{0,1:T(8,128)(2,1)S(1)}, u32[]{:S(2)}, u32[]{:S(2)}) %collective-permute-start.1) | collective-permute-done | bytes 720928 | tf_op jit(solution)/shard_map/ppermute | solution.py:42
  158.7 10.3 %collective-permute-done.2 = bf16[512,704]{0,1:T(8,128)(2,1)} collective-permute-done((bf16[512,704]{0,1:T(8,128)(2,1)S(1)}, bf16[512,704]{0,1:T(8,128)(2,1)}, u32[]{:S(2)}, u32[]{:S(2)}) %collective-permute-start.2) | collective-permute-done | bytes 720928 | tf_op jit(solution)/shard_map/ppermute | solution.py:42
  170.4 3.8 concatenate.40
  174.2 12.9 %all-gather.15.cloned.1.call-done = bf16[2816,512]{1,0:T(8,128)(2,1)} async-done(((bf16[352,512]{1,0:T(8,128)(2,1)}), bf16[2816,512]{1,0:T(8,128)(2,1)}) %all-gather.15.cloned.1.call-update) | async-done | bytes 2883600 | tf_op jit(solution)/shard_map/all_gather | solution.py:30
  187.1 6.1 fusion.48
  194.2 20.4 %all-gather.17.cloned.1.call-done = bf16[512,2048]{1,0:T(8,128)(2,1)} async-done(((bf16[512,512]{1,0:T(8,128)(2,1)}), bf16[512,2048]{1,0:T(8,128)(2,1)}) %all-gather.17.cloned.1.call-update) | async-done | bytes 2097168 | tf_op jit(solution)/shard_map/all_gather | solution.py:24
  216.7 49.0 %all-gather.19.cloned.1.call-done = bf16[2048,512]{1,0:T(8,128)(2,1)} async-done(((bf16[256,512]{1,0:T(8,128)(2,1)}), bf16[2048,512]{1,0:T(8,128)(2,1)}) %all-gather.19.cloned.1.call-update) | async-done | bytes 2097168 | tf_op jit(solution)/shard_map/all_gather | solution.py:30
  265.7 3.5 fusion.20
  272.6 9.1 %slice.212 = f32[4,64,256]{1,2,0:T(8,128)S(1)} slice(f32[4,128,256]{1,2,0:T(8,128)S(1)} %get-tuple-element.7), slice={[0:4:1], [0:127:2], [0:256:1]} | slice | bytes 524288 | tf_op jit(solution)/shard_map/slice | solution.py:90
  281.7 9.1 %slice.213 = f32[4,64,256]{1,2,0:T(8,128)S(1)} slice(f32[4,128,256]{1,2,0:T(8,128)S(1)} %get-tuple-element.7), slice={[0:4:1], [1:128:2], [0:256:1]} | slice | bytes 524288 | tf_op jit(solution)/shard_map/slice | solution.py:90
  290.7 9.1 %slice.211 = f32[4,64,256]{1,2,0:T(8,128)S(1)} slice(f32[4,128,256]{1,2,0:T(8,128)S(1)} %get-tuple-element.6), slice={[0:4:1], [1:128:2], [0:256:1]} | slice | bytes 524288 | tf_op jit(solution)/shard_map/slice | solution.py:90
  299.8 9.5 %slice.215 = f32[4,64,256]{1,2,0:T(8,128)} slice(f32[4,128,256]{1,2,0:T(8,128)S(1)} %get-tuple-element.6), slice={[0:4:1], [0:127:2], [0:256:1]} | slice | bytes 524288 | tf_op jit(solution)/shard_map/slice | solution.py:90
  310.5 4.6 slice.218
  315.1 4.7 slice.219
  319.8 5.3 slice.217
  325.2 5.2 slice.221
  331.7 2.5 slice.224
  334.1 3.2 slice.225
  337.3 3.4 slice.223
  340.7 3.1 slice.227
  345.2 2.3 slice.230
  347.5 2.4 slice.231
  349.9 2.4 slice.229
  352.2 2.3 slice.233
  363.8 2.4 fusion.96
  369.7 3.4 slice.241
  373.1 3.3 slice.245
  382.2 3.5 slice.234
  387.6 2.3 slice.228
  389.8 2.3 slice.253
  392.1 4.3 slice.222
  396.4 3.1 slice.255
  399.4 6.1 slice.216
  405.5 5.2 slice.257
  410.7 9.5 %slice.210 = f32[4,63,256]{1,2,0:T(8,128)} slice(f32[4,128,256]{1,2,0:T(8,128)S(1)} %copy-done.1), slice={[0:4:1], [2:128:2], [0:256:1]} | slice | bytes 516096 | tf_op jit(solution)/shard_map/slice | solution.py:90
  420.2 9.9 %slice.259 = f32[4,63,256]{1,2,0:T(8,128)} slice(f32[4,128,256]{1,2,0:T(8,128)S(1)} %get-tuple-element.7), slice={[0:4:1], [2:128:2], [0:256:1]} | slice | bytes 516096 | tf_op jit(solution)/shard_map/slice | solution.py:90
  434.8 2.2 pad.50
  437.0 4.3 pad.51
  443.2 2.5 pad.53
  445.6 2.2 add_multiply_fusion.4
  451.6 2.4 pad.52
  460.9 2.9 pad.55
  464.7 3.7 pad.57
  470.7 3.6 pad.56
  475.5 4.5 pad.58
  480.0 4.6 pad.59
  485.4 9.8 %pad.61 = f32[4,128,256]{1,2,0:T(8,128)S(1)} pad(f32[4,64,256]{1,2,0:T(8,128)} %add.208, f32[]{:T(128)} %constant.19.clone.1), padding=0_0_0x1_0_1x0_0_0 | pad | bytes 786436 | tf_op jit(solution)/shard_map/pad | solution.py:90
  495.7 8.8 %pad.60 = f32[4,128,256]{1,2,0:T(8,128)S(1)} pad(f32[4,64,256]{1,2,0:T(8,128)S(1)} %pad_maximum_fusion.4, f32[]{:T(128)} %constant.19.clone.1), padding=0_0_0x0_1_1x0_0_0 | pad | bytes 786436 | tf_op jit(solution)/shard_map/pad | solution.py:90
  506.5 14.7 %all-gather.21.cloned.1.call-done = bf16[512,1024]{1,0:T(8,128)(2,1)} async-done(((bf16[512,256]{1,0:T(8,128)(2,1)}), bf16[512,1024]{1,0:T(8,128)(2,1)}) %all-gather.21.cloned.1.call-update) | async-done | bytes 1048592 | tf_op jit(solution)/shard_map/all_gather | solution.py:94
  522.7 40.9 %all-gather.23.cloned.1.call-done = bf16[1024,512]{1,0:T(8,128)(2,1)} async-done(((bf16[128,512]{1,0:T(8,128)(2,1)}), bf16[1024,512]{1,0:T(8,128)(2,1)}) %all-gather.23.cloned.1.call-update) | async-done | bytes 1048592 | tf_op jit(solution)/shard_map/all_gather | solution.py:30
  563.6 3.1 fusion.44
  568.9 19.3 %all-gather.25.cloned.1.call-done = bf16[512,2048]{1,0:T(8,128)(2,1)} async-done(((bf16[512,512]{1,0:T(8,128)(2,1)}), bf16[512,2048]{1,0:T(8,128)(2,1)}) %all-gather.25.cloned.1.call-update) | async-done | bytes 2097168 | tf_op jit(solution)/shard_map/all_gather | solution.py:24
  590.3 93.1 %all-gather.27.cloned.1.call-done = bf16[2048,1408]{0,1:T(8,128)(2,1)} async-done(((bf16[256,1408]{0,1:T(8,128)(2,1)}), bf16[2048,1408]{0,1:T(8,128)(2,1)}) %all-gather.27.cloned.1.call-update) | async-done | bytes 5767184 | tf_op jit(solution)/shard_map/all_gather | solution.py:30
  683.4 6.5 fusion.18
  690.8 10.7 %collective-permute-done.3 = bf16[512,704]{0,1:T(8,128)(2,1)S(1)} collective-permute-done((bf16[512,704]{0,1:T(8,128)(2,1)S(1)}, bf16[512,704]{0,1:T(8,128)(2,1)S(1)}, u32[]{:S(2)}, u32[]{:S(2)}) %collective-permute-start.3) | collective-permute-done | bytes 720928 | tf_op jit(solution)/shard_map/ppermute | solution.py:42
  701.5 10.7 %collective-permute-done.4 = bf16[512,704]{0,1:T(8,128)(2,1)S(1)} collective-permute-done((bf16[512,704]{0,1:T(8,128)(2,1)S(1)}, bf16[512,704]{0,1:T(8,128)(2,1)S(1)}, u32[]{:S(2)}, u32[]{:S(2)}) %collective-permute-start.4) | collective-permute-done | bytes 720928 | tf_op jit(solution)/shard_map/ppermute | solution.py:42
  712.7 10.3 %collective-permute-done.5 = bf16[512,704]{0,1:T(8,128)(2,1)} collective-permute-done((bf16[512,704]{0,1:T(8,128)(2,1)S(1)}, bf16[512,704]{0,1:T(8,128)(2,1)}, u32[]{:S(2)}, u32[]{:S(2)}) %collective-permute-start.5) | collective-permute-done | bytes 720928 | tf_op jit(solution)/shard_map/ppermute | solution.py:42
  724.4 3.8 concatenate.49
  728.2 12.8 %all-gather.29.cloned.1.call-done = bf16[2816,512]{1,0:T(8,128)(2,1)} async-done(((bf16[352,512]{1,0:T(8,128)(2,1)}), bf16[2816,512]{1,0:T(8,128)(2,1)}) %all-gather.29.cloned.1.call-update) | async-done | bytes 2883600 | tf_op jit(solution)/shard_map/all_gather | solution.py:30
  740.9 6.1 fusion.45
  (179 shorter events, 73.5 us)
Async XLA Ops:
  6.5 4.1 copy-start.16
  6.5 27.7 %all-gather.11.cloned.1.call-start = ((), (), s32[]{:S(2)}) async-start(), calls=%async_computation | async-start | bytes 2621440 | tf_op jit(solution)/shard_map/all_gather | solution.py:24
  7.3 122.2 %all-gather.13.cloned.1.call-start = ((), (), s32[]{:S(2)}) async-start(), calls=%async_computation.1 | async-start | bytes 6488064 | tf_op jit(solution)/shard_map/all_gather | solution.py:30
  9.6 119.8 %copy-start.28 = (f32[2048]{0:T(1024)S(1)}, f32[2048]{0:T(1024)}, u32[]{:S(2)}) copy-start(f32[2048]{0:T(1024)} %param.21) | copy-start | bytes 24580
  10.6 176.6 %all-gather.15.cloned.1.call-start = ((), (), s32[]{:S(2)}) async-start(), calls=%async_computation.2 | async-start | bytes 3244032 | tf_op jit(solution)/shard_map/all_gather | solution.py:30
  11.4 203.2 %all-gather.17.cloned.1.call-start = ((), (), s32[]{:S(2)}) async-start(), calls=%async_computation.3 | async-start | bytes 2621440 | tf_op jit(solution)/shard_map/all_gather | solution.py:24
  136.7 10.8 %collective-permute-start = (bf16[512,704]{0,1:T(8,128)(2,1)S(1)}, bf16[512,704]{0,1:T(8,128)(2,1)S(1)}, u32[]{:S(2)}, u32[]{:S(2)}) collective-permute-start(bf16[512,704]{0,1:T(8,128)(2,1)S(1)} %copy.65), channel_id=1, source_target_pairs={{0,1},{1,2},{2,3},{3,0},{4,5},{5,6},{6,7},{7,4},{8,9},{9,10},{10,1... | collective-permute-start | bytes 2162696 | tf_op jit(solution)/shard_map/ppermute | solution.py:42
  147.5 10.7 %collective-permute-start.1 = (bf16[512,704]{0,1:T(8,128)(2,1)S(1)}, bf16[512,704]{0,1:T(8,128)(2,1)S(1)}, u32[]{:S(2)}, u32[]{:S(2)}) collective-permute-start(bf16[512,704]{0,1:T(8,128)(2,1)S(1)} %collective-permute-done), channel_id=1, source_target_pairs={{0,1},{1,2},{2,3},{3,0},{4,5},{5,6},{6,7},{7,4},{8,9},{9,10},{10,1... | collective-permute-start | bytes 2162696 | tf_op jit(solution)/shard_map/ppermute | solution.py:42
  158.2 10.8 %collective-permute-start.2 = (bf16[512,704]{0,1:T(8,128)(2,1)S(1)}, bf16[512,704]{0,1:T(8,128)(2,1)}, u32[]{:S(2)}, u32[]{:S(2)}) collective-permute-start(bf16[512,704]{0,1:T(8,128)(2,1)S(1)} %collective-permute-done.1), channel_id=1, source_target_pairs={{0,1},{1,2},{2,3},{3,0},{4,5},{5,6},{6,7},{7,4},{8,9},{9,10},{10,1... | collective-permute-start | bytes 2162696 | tf_op jit(solution)/shard_map/ppermute | solution.py:42
  174.2 19.1 %copy-start.21 = (f32[256,256]{1,0:T(8,128)S(1)}, f32[256,256]{1,0:T(8,128)}, u32[]{:S(2)}) copy-start(f32[256,256]{1,0:T(8,128)} %param.26) | copy-start | bytes 786436
  174.2 19.2 %copy-start.22 = (f32[256,256]{1,0:T(8,128)S(1)}, f32[256,256]{1,0:T(8,128)}, u32[]{:S(2)}) copy-start(f32[256,256]{1,0:T(8,128)} %param.27) | copy-start | bytes 786436
  174.2 20.0 %copy-start.25 = (f32[256]{0:T(256)S(1)}, f32[256]{0:T(256)}, u32[]{:S(2)}) copy-start(f32[256]{0:T(256)} %param.31) | copy-start | bytes 3076
  174.2 20.0 %copy-start.24 = (f32[4,256]{1,0:T(4,128)S(1)}, f32[4,256]{1,0:T(4,128)}, u32[]{:S(2)}) copy-start(f32[4,256]{1,0:T(4,128)} %param.28) | copy-start | bytes 12292
  193.2 72.5 %copy-start.29 = (f32[2048]{0:T(1024)S(1)}, f32[2048]{0:T(1024)}, u32[]{:S(2)}) copy-start(f32[2048]{0:T(1024)} %param.25) | copy-start | bytes 24580
  193.3 72.4 %all-gather.19.cloned.1.call-start = ((), (), s32[]{:S(2)}) async-start(), calls=%async_computation.4 | async-start | bytes 2359296 | tf_op jit(solution)/shard_map/all_gather | solution.py:30
  194.1 327.0 %all-gather.21.cloned.1.call-start = ((), (), s32[]{:S(2)}) async-start(), calls=%async_computation.5 | async-start | bytes 1310720 | tf_op jit(solution)/shard_map/all_gather | solution.py:94
  269.2 1.0 copy-start.14
  269.2 1.8 copy-start.26
  270.3 1.2 copy-start.27
  272.6 27.2 %copy-start = (f32[4,128,256]{1,2,0:T(8,128)}, f32[4,128,256]{1,2,0:T(8,128)S(1)}, u32[]{:S(2)}) copy-start(f32[4,128,256]{1,2,0:T(8,128)S(1)} %get-tuple-element.6) | copy-start | bytes 1572868
  310.5 14.7 %copy-start.2 = (f32[4,64,256]{1,2,0:T(8,128)}, f32[4,64,256]{1,2,0:T(8,128)S(1)}, u32[]{:S(2)}) copy-start(f32[4,64,256]{1,2,0:T(8,128)S(1)} %get-tuple-element.20) | copy-start | bytes 786436
  331.7 9.0 %copy-start.3 = (f32[4,32,256]{1,2,0:T(8,128)}, f32[4,32,256]{1,2,0:T(8,128)S(1)}, u32[]{:S(2)}) copy-start(f32[4,32,256]{1,2,0:T(8,128)S(1)} %get-tuple-element.18) | copy-start | bytes 393220
  345.2 7.0 copy-start.4
  356.2 5.8 copy-start.6
  376.4 3.2 copy-start.7
  381.3 6.3 copy-start.5
  389.8 20.8 %copy-start.1 = (f32[4,128,256]{1,2,0:T(8,128)S(1)}, f32[4,128,256]{1,2,0:T(8,128)}, u32[]{:S(2)}) copy-start(f32[4,128,256]{1,2,0:T(8,128)} %copy-done) | copy-start | bytes 1572868
  437.0 4.3 copy-start.8
  469.7 5.5 copy-start.11
  469.7 5.5 copy-start.12
  475.2 4.7 copy-start.13
  475.2 20.1 %copy-start.9 = (f32[4,63,256]{1,2,0:T(8,128)S(1)}, f32[4,63,256]{1,2,0:T(8,128)}, u32[]{:S(2)}) copy-start(f32[4,63,256]{1,2,0:T(8,128)} %slice.210) | copy-start | bytes 774148
  475.3 20.1 %copy-start.10 = (f32[4,63,256]{1,2,0:T(8,128)S(1)}, f32[4,63,256]{1,2,0:T(8,128)}, u32[]{:S(2)}) copy-start(f32[4,63,256]{1,2,0:T(8,128)} %slice.259) | copy-start | bytes 774148
  495.4 9.3 %copy-start.15 = (f32[512,512]{1,0:T(8,128)S(1)}, f32[512,512]{1,0:T(8,128)}, u32[]{:S(2)}) copy-start(f32[512,512]{1,0:T(8,128)} %copy-done.14) | copy-start | bytes 3145732
  495.6 10.1 %copy-start.23 = (f32[128,512]{1,0:T(8,128)S(1)}, f32[128,512]{1,0:T(8,128)}, u32[]{:S(2)}) copy-start(f32[128,512]{1,0:T(8,128)} %param.33) | copy-start | bytes 786436
  504.5 59.2 %copy-start.31 = (f32[1024]{0:T(1024)S(1)}, f32[1024]{0:T(1024)}, u32[]{:S(2)}) copy-start(f32[1024]{0:T(1024)} %param.32) | copy-start | bytes 12292
  504.5 59.1 %copy-start.20 = (bf16[512,512]{1,0:T(8,128)(2,1)S(1)}, bf16[512,512]{1,0:T(8,128)(2,1)}, u32[]{:S(2)}) copy-start(bf16[512,512]{1,0:T(8,128)(2,1)} %fusion.48) | copy-start | bytes 1572868
  505.7 57.9 %all-gather.23.cloned.1.call-start = ((), (), s32[]{:S(2)}) async-start(), calls=%async_computation.6 | async-start | bytes 1179648 | tf_op jit(solution)/shard_map/all_gather | solution.py:30
  506.4 60.5 %copy-start.17 = (f32[256,704]{0,1:T(8,128)S(1)}, f32[256,704]{0,1:T(8,128)}, u32[]{:S(2)}) copy-start(f32[256,704]{0,1:T(8,128)} %param.35) | copy-start | bytes 2162692
  506.5 81.7 %all-gather.25.cloned.1.call-start = ((), (), s32[]{:S(2)}) async-start(), calls=%async_computation.7 | async-start | bytes 2621440 | tf_op jit(solution)/shard_map/all_gather | solution.py:24
  522.7 44.3 %copy-start.18 = (f32[256,704]{0,1:T(8,128)S(1)}, f32[256,704]{0,1:T(8,128)}, u32[]{:S(2)}) copy-start(f32[256,704]{0,1:T(8,128)} %param.36) | copy-start | bytes 2162692
  566.7 1.4 copy-start.19
  566.7 116.7 %all-gather.27.cloned.1.call-start = ((), (), s32[]{:S(2)}) async-start(), calls=%async_computation.8 | async-start | bytes 6488064 | tf_op jit(solution)/shard_map/all_gather | solution.py:30
  567.1 116.3 %copy-start.30 = (f32[2048]{0:T(1024)S(1)}, f32[2048]{0:T(1024)}, u32[]{:S(2)}) copy-start(f32[2048]{0:T(1024)} %param.34) | copy-start | bytes 24580
  568.0 172.9 %all-gather.29.cloned.1.call-start = ((), (), s32[]{:S(2)}) async-start(), calls=%async_computation.9 | async-start | bytes 3244032 | tf_op jit(solution)/shard_map/all_gather | solution.py:30
  690.7 10.8 %collective-permute-start.3 = (bf16[512,704]{0,1:T(8,128)(2,1)S(1)}, bf16[512,704]{0,1:T(8,128)(2,1)S(1)}, u32[]{:S(2)}, u32[]{:S(2)}) collective-permute-start(bf16[512,704]{0,1:T(8,128)(2,1)S(1)} %copy.90), channel_id=1, source_target_pairs={{0,1},{1,2},{2,3},{3,0},{4,5},{5,6},{6,7},{7,4},{8,9},{9,10},{10,1... | collective-permute-start | bytes 2162696 | tf_op jit(solution)/shard_map/ppermute | solution.py:42
  701.5 10.7 %collective-permute-start.4 = (bf16[512,704]{0,1:T(8,128)(2,1)S(1)}, bf16[512,704]{0,1:T(8,128)(2,1)S(1)}, u32[]{:S(2)}, u32[]{:S(2)}) collective-permute-start(bf16[512,704]{0,1:T(8,128)(2,1)S(1)} %collective-permute-done.3), channel_id=1, source_target_pairs={{0,1},{1,2},{2,3},{3,0},{4,5},{5,6},{6,7},{7,4},{8,9},{9,10},{10,1... | collective-permute-start | bytes 2162696 | tf_op jit(solution)/shard_map/ppermute | solution.py:42
  712.2 10.8 %collective-permute-start.5 = (bf16[512,704]{0,1:T(8,128)(2,1)S(1)}, bf16[512,704]{0,1:T(8,128)(2,1)}, u32[]{:S(2)}, u32[]{:S(2)}) collective-permute-start(bf16[512,704]{0,1:T(8,128)(2,1)S(1)} %collective-permute-done.4), channel_id=1, source_target_pairs={{0,1},{1,2},{2,3},{3,0},{4,5},{5,6},{6,7},{7,4},{8,9},{9,10},{10,1... | collective-permute-start | bytes 2162696 | tf_op jit(solution)/shard_map/ppermute | solution.py:42
Sparse Core Ops, SparseCore 0:
  8.9 25.2 all-gather.10
  36.3 93.1 all-gather.12
  131.6 55.4 all-gather.14
  193.4 21.1 all-gather.16
  216.6 49.0 all-gather.18
  505.8 15.3 all-gather.20
  523.3 40.2 all-gather.22
  566.9 21.2 all-gather.24
  590.2 93.1 all-gather.26
  685.4 55.4 all-gather.28
